TPU v7x, 32 devices: a whole 2x2x4 slice. The times are simulated.
32 devices in a mesh: tp: 8 (over z, core), dp: 4 (over y, x).
Axes of the slice: x: 2, y: 2, z: 4, core: 2. Of those that a mesh axis runs over, the one named last changes fastest.
Arguments:
- incoming_embeddings: bfloat16 [24, 4096], P('tp', 'dp'), may hold values from -12 to 12
- rescale_factors: bfloat16 [2, 4096], P(None, 'dp'), may hold values from 0.099609375 to 1.8984375
- probe_lift: bfloat16 [2, 4096, 4096], P(None, 'dp', 'tp'), may hold values from -0.09375 to 0.09375
- address_lift: bfloat16 [2, 4096, 4096], P(None, 'dp', 'tp'), may hold values from -0.09375 to 0.09375
- forget_lift: bfloat16 [2, 4096, 4096], P(None, 'dp', 'tp'), may hold values from -0.09375 to 0.09375
- forget_shift: float32 [2, 4096], P(None, 'tp'), may hold values from -6 to 3
- surplus_fade: float32 [2, 24, 4096], P(None, 'dp', 'tp'), may hold values from -0.7 to 0
- content_lift: bfloat16 [2, 4096, 8192], P(None, 'dp', 'tp'), may hold values from -0.09375 to 0.09375
- filter_lift: bfloat16 [2, 4096, 8192], P(None, 'dp', 'tp'), may hold values from -0.09375 to 0.09375
- readback_lift: bfloat16 [2, 8192, 4096], P(None, 'tp', 'dp'), may hold values from -0.0625 to 0.0625
- memory_tensor: float32 [2, 24, 128, 8192], P(None, 'dp', None, 'tp'), may hold values from -6 to 6
Outputs:
- mixed: bfloat16 [24, 4096], P('tp', 'dp')
- new_state: float32 [2, 24, 128, 8192], P(None, 'dp', None, 'tp')
All inputs are finite; a program needn't handle non-finite values.
Results may differ from a plain program's by a relative error of at most 0.0085.
Values may be sent and summed in bfloat16 or wider, within the bound.
A program may use at most 128 MiB of HBM per device.

v0:
```python
import jax
import jax.numpy as jnp
from jax import lax
from jax.sharding import PartitionSpec as P

D = 4096
DK = 128
BLOCKS = 2


def shards(
    incoming_embeddings,
    rescale_factors,
    probe_lift,
    address_lift,
    forget_lift,
    forget_shift,
    surplus_fade,
    content_lift,
    filter_lift,
    readback_lift,
    memory_tensor,
):
    key_cols = probe_lift.shape[2]
    value_cols = content_lift.shape[2]
    seq_local = memory_tensor.shape[1]
    heads_here = key_cols // DK
    head_width = value_cols // heads_here
    stream = incoming_embeddings
    collected = []
    for layer_ordinal in range(BLOCKS):
        resid = stream.astype(jnp.float32)
        gain_cols = rescale_factors[layer_ordinal].astype(jnp.float32)
        matrices = jnp.concatenate(
            [
                probe_lift[layer_ordinal],
                address_lift[layer_ordinal],
                forget_lift[layer_ordinal],
                content_lift[layer_ordinal],
                filter_lift[layer_ordinal],
            ],
            axis=1,
        )
        all_rows = lax.all_gather(stream, "tp", axis=0, tiled=True)
        all_float = all_rows.astype(jnp.float32)
        hidden = (all_float * gain_cols).astype(jnp.bfloat16)
        row_squares = jnp.sum(all_float * all_float, axis=1)
        projected = lax.psum_scatter(
            jnp.dot(hidden, matrices, preferred_element_type=jnp.float32),
            "dp",
            scatter_dimension=0,
            tiled=True,
        )
        total_squares = lax.psum(row_squares, "dp")
        own_squares = lax.dynamic_slice_in_dim(
            total_squares, lax.axis_index("dp") * seq_local, seq_local, 0
        )
        inv_rms = lax.rsqrt(own_squares / D + 1e-06)[:, None]
        projected = projected * inv_rms
        queries = projected[:, :key_cols] * DK ** (-0.5)
        key_vals = projected[:, key_cols : 2 * key_cols]
        forget_preact = projected[:, 2 * key_cols : 3 * key_cols] + forget_shift[layer_ordinal]
        values = projected[:, 3 * key_cols : 3 * key_cols + value_cols]
        gate_vals = projected[:, 3 * key_cols + value_cols :]
        forget_rate_ln = jax.nn.log_sigmoid(forget_preact) / 16.0 + surplus_fade[layer_ordinal]
        old_state = memory_tensor[layer_ordinal].reshape(seq_local, DK, heads_here, head_width)
        decays = jnp.transpose(
            jnp.exp(forget_rate_ln).reshape(seq_local, heads_here, DK), (0, 2, 1)
        )
        key_heads = key_vals.reshape(seq_local, heads_here, DK)
        value_heads = values.reshape(seq_local, heads_here, head_width)
        fresh = old_state * decays[..., None] + jnp.einsum(
            "shk,she->skhe", key_heads, value_heads, precision=lax.Precision.HIGHEST
        )
        readout = jnp.einsum(
            "shk,skhe->she",
            queries.reshape(seq_local, heads_here, DK),
            fresh,
            precision=lax.Precision.HIGHEST,
        ).reshape(seq_local, value_cols)
        gated = (readout * jax.nn.silu(gate_vals)).astype(jnp.bfloat16)
        out_block = readback_lift[layer_ordinal]
        branch_all = jnp.dot(
            lax.all_gather(gated, "dp", axis=0, tiled=True),
            out_block,
            preferred_element_type=jnp.float32,
        )
        branch = lax.psum_scatter(branch_all, "tp", scatter_dimension=0, tiled=True)
        stream = (resid + branch).astype(jnp.bfloat16)
        collected.append(fresh.reshape(seq_local, DK, value_cols))
    return (stream, jnp.stack(collected))


def solution(mesh):
    in_specs = (
        P("tp", "dp"),
        P(None, "dp"),
        P(None, "dp", "tp"),
        P(None, "dp", "tp"),
        P(None, "dp", "tp"),
        P(None, "tp"),
        P(None, "dp", "tp"),
        P(None, "dp", "tp"),
        P(None, "dp", "tp"),
        P(None, "tp", "dp"),
        P(None, "dp", None, "tp"),
    )
    out_specs = (P("tp", "dp"), P(None, "dp", None, "tp"))
    return jax.shard_map(shards, mesh=mesh, in_specs=in_specs, out_specs=out_specs, check_vma=False)
```

profile of v0, /device:TPU:0, one launch (start us, length us, event | category | flops | bytes accessed | tf_op | source)
XLA Modules:
  0.0 310.7 jit_solution(7896688341757499493)
XLA Ops:
  7.2 0.0 all-reduce.9.cloned.1.call-start
  7.2 3.2 %bitcast_dynamic-update-slice_fusion.9 = (bf16[1024,3584]{1,0:T(8,128)(2,1)}, bf16[1024,3584]{1,0:T(8,128)(2,1)}) fusion(bf16[2,1024,512]{2,1,0:T(8,128)(2,1)} %param.13), kind=kLoop, calls=%fused_computation.22 | loop fusion | bytes 4194304
  10.5 15.7 %all-gather = bf16[8,3,1024]{2,1,0:T(4,128)(2,1)S(1)} all-gather(bf16[1,3,1024]{2,1,0:T(4,128)(2,1)S(1)} %bitcast.79), channel_id=1, replica_groups=mesh['tp'=8,'dp'=4] {'tp'}, dimensions={0}, use_global_device_ids=true | all-gather | bytes 55296 | tf_op jit(solution)/shard_map/all_gather | solution.py:44
  26.2 0.0 copy-start.3
  26.2 1.5 bitcast_dynamic-update-slice_fusion.8
  27.7 0.8 copy-done.3
  28.5 1.5 bitcast_dynamic-update-slice_fusion.7
  30.1 2.6 bitcast_dynamic-update-slice_fusion.3
  32.6 1.1 copy-done.1
  33.8 2.5 bitcast_dynamic-update-slice_fusion.2
  36.3 4.9 %fusion.10 = f32[24,3584]{1,0:T(8,128)} fusion(bf16[1024,3584]{1,0:T(8,128)(2,1)} %get-tuple-element.4, f32[24,1024]{1,0:T(8,128)S(1)} %reshape.58, f32[1024]{0:T(1024)S(1)} %bitcast.85), kind=kOutput, calls=%fused_computation.29 | convolution fusion | flops 176209920 | bytes 7786496 | tf_op jit(solution)/shard_map/dot_general | solution.py:49
  41.2 0.0 all-reduce.9.cloned.1.call-update
  41.2 0.0 all-reduce.11.cloned.1.call-start
  41.3 0.1 multiply_reduce_fusion.1
  41.4 5.4 %fusion.29 = (f32[1,6,128,1024]{3,2,1,0:T(8,128)}, f32[1,6,128,1024]{3,2,1,0:T(8,128)S(1)}) fusion(f32[2,6,128,1024]{3,2,1,0:T(8,128)} %param.21), kind=kLoop, calls=%fused_computation.66 | loop fusion | bytes 12582912 | tf_op jit(solution)/shard_map/slice | solution.py:66
  46.8 9.9 %psum.14 = f32[24]{0:T(128)S(1)} all-reduce(f32[24]{0:T(128)S(1)} %multiply_reduce_fusion.1), channel_id=1, replica_groups=mesh['tp'=8,'dp'=4] {'dp'}, use_global_device_ids=true, to_apply=%region_2.0 | all-reduce | flops 24 | bytes 192 | tf_op jit(solution)/shard_map/psum | solution.py:54
  56.7 2.9 reshape_squeeze.6
  59.6 0.6 dynamic-slice
  60.9 0.1 add_rsqrt_fusion.1
  61.0 0.6 fusion.30
  61.6 24.6 %all-reduce.9.cloned.1.call-done = f32[24,3584]{1,0:T(8,128)} async-done(((f32[24,3584]{1,0:T(8,128)}), f32[24,3584]{1,0:T(8,128)}) %all-reduce.9.cloned.1.call-update) | async-done | bytes 344080
  86.2 1.0 dynamic-slice_multiply_fusion.1
  87.2 0.6 copy-done.5
  87.9 0.2 copy.26
  88.1 1.0 copy.27
  89.1 0.6 reshape.40
  89.7 0.6 reshape.60
  90.3 3.9 %bitcast_add_fusion.1 = f32[6,128,4,256]{3,2,1,0:T(4,128)S(1)} fusion(f32[6,128,4,256]{3,2,1,0:T(4,128)} %reshape_squeeze.6, f32[6,4,128]{1,2,0:T(8,128)} %copy.27, f32[6,4,256]{2,1,0:T(4,128)} %reshape.40, f32[6,128,4]{2,1,0:T(8,128)S(1)} %copy.26), kind=kLoop, calls=%fused_computation.2 | loop fusion | flops 2359296 | bytes 6340608 | tf_op jit(solution)/shard_map/add | solution.py:72
  94.2 0.0 copy-start.13
  94.2 2.0 fusion.2
  96.2 0.8 fusion.26
  97.0 8.2 %all-gather.1 = bf16[4,6,1024]{2,1,0:T(8,128)(2,1)S(1)} all-gather(bf16[1,6,1024]{2,1,0:T(8,128)(2,1)S(1)} %fusion.26), channel_id=1, replica_groups=mesh['tp'=8,'dp'=4] {'dp'}, dimensions={0}, use_global_device_ids=true | all-gather | bytes 61440 | tf_op jit(solution)/shard_map/all_gather | solution.py:84
  105.2 2.6 fusion.6
  107.8 0.0 all-reduce.11.cloned.1.call-update
  107.9 0.0 all-reduce.13.cloned.1.call-start
  107.9 0.6 dynamic-slice.2
  109.2 51.2 %all-reduce.11.cloned.1.call-done = f32[24,1024]{1,0:T(8,128)} async-done(((f32[24,1024]{1,0:T(8,128)}), f32[24,1024]{1,0:T(8,128)}) %all-reduce.11.cloned.1.call-update) | async-done | bytes 98320
  160.4 0.8 fusion.28
  161.2 15.7 %all-gather.2 = bf16[8,3,1024]{2,1,0:T(4,128)(2,1)S(1)} all-gather(bf16[1,3,1024]{2,1,0:T(4,128)(2,1)S(1)} %fusion.28), channel_id=1, replica_groups=mesh['tp'=8,'dp'=4] {'tp'}, dimensions={0}, use_global_device_ids=true | all-gather | bytes 55296 | tf_op jit(solution)/shard_map/all_gather | solution.py:44
  176.9 4.9 %fusion.11 = f32[24,3584]{1,0:T(8,128)} fusion(bf16[1024,3584]{1,0:T(8,128)(2,1)} %get-tuple-element.5, f32[24,1024]{1,0:T(8,128)S(1)} %reshape.59, f32[1024]{0:T(1024)S(1)} %bitcast.84), kind=kOutput, calls=%fused_computation.30 | convolution fusion | flops 176209920 | bytes 7786496 | tf_op jit(solution)/shard_map/dot_general | solution.py:49
  181.8 0.0 all-reduce.13.cloned.1.call-update
  181.8 0.0 all-reduce.15.cloned.1.call-start
  181.9 5.2 %reshape_squeeze.7 = f32[6,128,4,256]{3,2,1,0:T(4,128)} reshape(f32[1,6,128,1024]{3,2,1,0:T(8,128)} %get-tuple-element.2) | data formatting | bytes 6291456 | tf_op jit(solution)/shard_map/reshape;squeeze | solution.py:66
  187.1 0.1 multiply_reduce_fusion
  187.2 3.0 stack_reshape.6
  190.2 10.1 %psum.15 = f32[24]{0:T(128)S(1)} all-reduce(f32[24]{0:T(128)S(1)} %multiply_reduce_fusion), channel_id=1, replica_groups=mesh['tp'=8,'dp'=4] {'dp'}, use_global_device_ids=true, to_apply=%region_6.7 | all-reduce | flops 24 | bytes 192 | tf_op jit(solution)/shard_map/psum | solution.py:54
  200.3 0.1 add_rsqrt_fusion
  200.4 25.1 %all-reduce.13.cloned.1.call-done = f32[24,3584]{1,0:T(8,128)} async-done(((f32[24,3584]{1,0:T(8,128)}), f32[24,3584]{1,0:T(8,128)}) %all-reduce.13.cloned.1.call-update) | async-done | bytes 344080
  225.5 1.0 dynamic-slice_multiply_fusion
  226.5 0.6 copy-done.4
  227.2 0.6 fusion.21
  227.8 0.2 copy.29
  228.0 0.9 copy.30
  228.9 0.6 reshape.45
  229.5 3.8 %bitcast_add_fusion = f32[6,128,4,256]{3,2,1,0:T(4,128)S(1)} fusion(f32[6,128,4,256]{3,2,1,0:T(4,128)} %reshape_squeeze.7, f32[6,4,128]{1,2,0:T(8,128)} %copy.30, f32[6,4,256]{2,1,0:T(4,128)} %reshape.45, f32[6,128,4]{2,1,0:T(8,128)S(1)} %copy.29), kind=kLoop, calls=%fused_computation.1 | loop fusion | flops 2359296 | bytes 6340608 | tf_op jit(solution)/shard_map/add | solution.py:72
  233.4 3.1 stack_reshape.7
  236.5 2.0 fusion
  238.5 0.8 fusion.27
  239.3 8.2 %all-gather.3 = bf16[4,6,1024]{2,1,0:T(8,128)(2,1)S(1)} all-gather(bf16[1,6,1024]{2,1,0:T(8,128)(2,1)S(1)} %fusion.27), channel_id=1, replica_groups=mesh['tp'=8,'dp'=4] {'dp'}, dimensions={0}, use_global_device_ids=true | all-gather | bytes 61440 | tf_op jit(solution)/shard_map/all_gather | solution.py:84
  247.5 2.6 fusion.4
  250.2 0.0 all-reduce.15.cloned.1.call-update
  250.2 6.7 %pad_maximum_fusion = f32[2,6,128,1024]{3,2,1,0:T(8,128)} fusion(f32[1,6,128,1024]{3,2,1,0:T(8,128)} %stack_reshape.7, f32[1,6,128,1024]{3,2,1,0:T(8,128)} %stack_reshape.6), kind=kLoop, calls=%fused_computation | loop fusion | flops 1572864 | bytes 12582912 | tf_op jit(solution)/shard_map/stack | solution.py:91
  256.9 45.8 %all-reduce.15.cloned.1.call-done = f32[24,1024]{1,0:T(8,128)} async-done(((f32[24,1024]{1,0:T(8,128)}), f32[24,1024]{1,0:T(8,128)}) %all-reduce.15.cloned.1.call-update) | async-done | bytes 98320
  302.7 1.5 fusion.24
  (42 shorter events, 0.3 us)
Async XLA Ops:
  7.2 3.3 %copy-start.6 = (bf16[3,1024]{1,0:T(4,128)(2,1)S(1)}, bf16[3,1024]{1,0:T(4,128)(2,1)}, u32[]{:S(2)}) copy-start(bf16[3,1024]{1,0:T(4,128)(2,1)} %param.11) | copy-start | bytes 18436
  7.2 19.0 %copy-start.11 = (bf16[2,1024]{1,0:T(2,128)(2,1)S(1)}, bf16[2,1024]{1,0:T(2,128)(2,1)}, u32[]{:S(2)}) copy-start(bf16[2,1024]{1,0:T(2,128)(2,1)} %param.12) | copy-start | bytes 12292
  7.2 19.0 %copy-start.2 = (bf16[2,1024,512]{2,1,0:T(8,128)(2,1)S(1)}, bf16[2,1024,512]{2,1,0:T(8,128)(2,1)}, u32[]{:S(2)}) copy-start(bf16[2,1024,512]{2,1,0:T(8,128)(2,1)} %param.14) | copy-start | bytes 6291460
  7.2 79.0 %all-reduce.9.cloned.1.call-start = ((), (), s32[]{:S(2)}) async-start(), calls=%async_computation | async-start | bytes 688128
  26.2 2.4 copy-start.3
  26.2 3.8 %copy-start = (bf16[2,1024,1024]{2,1,0:T(8,128)(2,1)S(1)}, bf16[2,1024,1024]{2,1,0:T(8,128)(2,1)}, u32[]{:S(2)}) copy-start(bf16[2,1024,1024]{2,1,0:T(8,128)(2,1)} %param.18) | copy-start | bytes 12582916
  30.1 3.7 %copy-start.1 = (bf16[2,1024,1024]{2,1,0:T(8,128)(2,1)S(1)}, bf16[2,1024,1024]{2,1,0:T(8,128)(2,1)}, u32[]{:S(2)}) copy-start(bf16[2,1024,1024]{2,1,0:T(8,128)(2,1)} %param.19) | copy-start | bytes 12582916
  41.2 119.2 %all-reduce.11.cloned.1.call-start = ((), (), s32[]{:S(2)}) async-start(), calls=%async_computation.1 | async-start | bytes 196608
  41.4 5.4 %copy-start.12 = (f32[2,512]{1,0:T(2,128)S(1)}, f32[2,512]{1,0:T(2,128)}, u32[]{:S(2)}) copy-start(f32[2,512]{1,0:T(2,128)} %param.16) | copy-start | bytes 12292
  46.8 12.9 %copy-start.14 = (u32[32]{0:T(128)S(1)}, u32[32]{0:T(128)}, u32[]{:S(2)}) copy-start(u32[32]{0:T(128)} %constant.37) | copy-start | bytes 388
  46.8 14.2 %copy-start.10 = (f32[2,6,512]{2,0,1:T(2,128)S(1)}, f32[2,6,512]{2,0,1:T(2,128)}, u32[]{:S(2)}) copy-start(f32[2,6,512]{2,0,1:T(2,128)} %param.17) | copy-start | bytes 73732
  87.2 0.6 copy-start.5
  90.3 3.9 %copy-start.8 = (f32[6,4,128,1]{2,1,0,3:T(4,128)S(1)}, f32[6,4,128,1]{2,1,0,3:T(4,128)}, u32[]{:S(2)}) copy-start(f32[6,4,128,1]{2,1,0,3:T(4,128)} %reshape.60) | copy-start | bytes 36868
  94.2 13.7 %copy-start.13 = (u32[32]{0:T(128)S(1)}, u32[32]{0:T(128)}, u32[]{:S(2)}) copy-start(u32[32]{0:T(128)} %constant.41) | copy-start | bytes 388
  107.9 117.6 %all-reduce.13.cloned.1.call-start = ((), (), s32[]{:S(2)}) async-start(), calls=%async_computation.2 | async-start | bytes 688128
  181.8 120.9 %all-reduce.15.cloned.1.call-start = ((), (), s32[]{:S(2)}) async-start(), calls=%async_computation.3 | async-start | bytes 196608
  187.1 40.1 %copy-start.9 = (f32[1,6,512]{2,0,1:T(1,128)S(1)}, f32[1,6,512]{2,0,1:T(1,128)}, u32[]{:S(2)}) copy-start(f32[1,6,512]{2,0,1:T(1,128)} %get-tuple-element.20) | copy-start | bytes 36868
  226.5 0.6 copy-start.4
  233.4 3.1 %copy-start.7 = (f32[6,512]{1,0:T(8,128)S(1)}, f32[6,512]{1,0:T(8,128)}, u32[]{:S(2)}) copy-start(f32[6,512]{1,0:T(8,128)} %get-tuple-element.16) | copy-start | bytes 36868
Sparse Core Ops, SparseCore 0:
  41.3 44.8 all-reduce.8
  108.0 52.3 all-reduce.10
  182.0 43.5 all-reduce.12
  250.3 52.3 all-reduce.14
where the time goes:
time: 312 us; the launch traced here: 311 us
  waiting for transfers between devices  147 us (47%)
  blocking collectives  67.8 us (22%)
  local copies, waits for them, and re-layouts  40.3 us (13%)
  other arithmetic  21.4 us (7%)
  matrix products  19 us (6%)
  between operations  15.3 us (5%)
    unnamed x8, waiting for transfers between devices  147 us
    all_gather x2, blocking collectives, shards(): all_rows = lax.all_gather(stream, 'tp', axis=0, tiled=True)  31.3 us
    psum x2, blocking collectives, shards(): total_squares = lax.psum(row_squares, 'dp')  20 us
    all_gather x2, blocking collectives, shards(): lax.all_gather(gated, 'dp', axis=0, tiled=True)  16.4 us
    unnamed x40, local copies, waits for them, and re-layouts  13.3 us
    dot_general x2, matrix products, shards(): jnp.dot(hidden, matrices, preferred_element_type=jnp.float32)  9.81 us
    another operation x2, local copies, waits for them, and re-layouts, shards(): memory_tensor[layer_ordinal].reshape(seq_local, DK, heads_here, head_width)  8.11 us
    add x2, other arithmetic, shards(): old_state * decays[..., None]  7.71 us
  transfers between devices with their start and end apart: 4, of which 4 were waited for; matrix products, arithmetic and copies ran while one was open for 8% of the time, Pallas kernels for 0%

commit v1 on v0

v1 whole, which is shorter than its diff:
```python
import functools

import jax
import jax.numpy as jnp
from jax import lax
from jax.experimental import pallas as pl
from jax.experimental.pallas import tpu as pltpu
from jax.sharding import PartitionSpec as P

DK = 128
BLOCKS = 2
SUB = 8
LANES = 128
LINK = jnp.bfloat16
F32 = jnp.float32


def kernel(
    n_tp, n_dp, x_hbm, gain_hbm, q_hbm, k_hbm, f_hbm, shift_hbm, fade_hbm, v_hbm, g_hbm, o_hbm, state_hbm,
    mixed_ref, out_hbm,
    gain, shift, fade, wq, wk, wf, wv, wg, wo, state,
    xg, hid, send_b, recv_b, cols, vals, readout, gated_all, part, send_e, recv_e,
    misc_sem, w_sem, out_sem, a_send, a_recv, b_send, b_recv, d_send, d_recv, e_send, e_recv,
):
    tp = lax.axis_index("tp")
    dp = lax.axis_index("dp")
    rows_tp = x_hbm.shape[0]
    depth = x_hbm.shape[1]
    kc = q_hbm.shape[2]
    vc = v_hbm.shape[2]
    seqs = state_hbm.shape[1]
    heads = kc // DK
    dv = vc // heads
    per = seqs // rows_tp
    pad = hid.shape[0] // n_dp
    model = depth * n_dp

    def peer_tp(o):
        return lax.rem(tp + o, n_tp)

    def peer_dp(o):
        return lax.rem(dp + o, n_dp)

    weights = [(f_hbm, wf), (k_hbm, wk), (q_hbm, wq), (v_hbm, wv), (g_hbm, wg), (o_hbm, wo), (state_hbm, state)]

    def load(b, i):
        src, dst = weights[i]
        return pltpu.make_async_copy(src.at[b], dst.at[b], w_sem.at[b, i])

    misc = [
        pltpu.make_async_copy(x_hbm, xg.at[0, tp], misc_sem.at[0]),
        pltpu.make_async_copy(gain_hbm, gain, misc_sem.at[1]),
        pltpu.make_async_copy(shift_hbm, shift, misc_sem.at[2]),
        pltpu.make_async_copy(fade_hbm, fade, misc_sem.at[3]),
    ]
    misc[0].start()
    misc[1].start()
    for i in range(5):
        load(0, i).start()
    misc[2].start()
    misc[3].start()

    barrier = pltpu.get_barrier_semaphore()
    for o in range(1, n_tp):
        pl.semaphore_signal(barrier, inc=1, device_id={"tp": peer_tp(o)}, device_id_type=pl.DeviceIdType.MESH)
    for o in range(1, n_dp):
        pl.semaphore_signal(barrier, inc=1, device_id={"dp": peer_dp(o)}, device_id_type=pl.DeviceIdType.MESH)
    hid[...] = jnp.zeros_like(hid)
    readout[...] = jnp.zeros_like(readout)
    misc[0].wait()
    misc[1].wait()
    pl.semaphore_wait(barrier, n_tp + n_dp - 2)

    def remote(src, dst, ss, rs, axis, target):
        return pltpu.make_async_remote_copy(
            src_ref=src, dst_ref=dst, send_sem=ss, recv_sem=rs,
            device_id={axis: target}, device_id_type=pl.DeviceIdType.MESH,
        )

    sent = []
    stored = []
    resid = None
    for b in range(BLOCKS):
        for o in range(1, n_tp):
            c = remote(xg.at[b, tp], xg.at[b, tp], a_send.at[b, o], a_recv.at[b, o], "tp", peer_tp(o))
            c.start()
            sent.append(c)
        if resid is None:
            resid = xg[b, tp].astype(F32)
        for o in range(1, n_tp):
            src = lax.rem(tp + n_tp - o, n_tp)
            remote(xg.at[b, src], xg.at[b, src], a_send.at[b, o], a_recv.at[b, o], "tp", src).wait_recv()
        for i in range(n_tp):
            at = pad * (i // per) + rows_tp * (i % per)
            hid[at:at + rows_tp, :] = xg[b, i].astype(F32)
        full = hid[...]
        squares = jnp.sum(full * full, axis=1, keepdims=True)
        hidden = (full * gain[b:b + 1, :].astype(F32)).astype(jnp.bfloat16)

        sq_hi = squares.astype(LINK).astype(F32)
        sq_lo = squares - sq_hi

        def put(value, at):
            for d in range(n_dp):
                send_b[b, d, :, at:at + value.shape[1]] = value[pad * d:pad * (d + 1)].astype(LINK)

        put(jnp.broadcast_to(sq_hi, (pad * n_dp, LANES)), 3 * kc)
        put(jnp.broadcast_to(sq_lo, (pad * n_dp, LANES)), 3 * kc + LANES)
        first = 3 * kc + 2 * LANES
        chunks = [(0, first, (0, 1, 2)), (first, vc, (3,)), (first + vc, vc, (4,))]
        for c, (start, width, members) in enumerate(chunks):
            at = start
            for m in members:
                load(b, m).wait()
                w = weights[m][1]
                put(jnp.dot(hidden, w[b], preferred_element_type=F32), at)
                at += w.shape[2]
            for o in range(1, n_dp):
                copy = remote(
                    send_b.at[b, peer_dp(o), :, pl.ds(start, width)],
                    recv_b.at[b, o - 1, :, pl.ds(start, width)],
                    b_send.at[b, c, o], b_recv.at[b, c, o], "dp", peer_dp(o),
                )
                copy.start()
                sent.append(copy)
            if b == 0 and c == 0:
                load(b, 6).start()
                load(b, 5).start()
        if b == 0:
            misc[2].wait()
            misc[3].wait()
        if b + 1 < BLOCKS:
            for i in (0, 1, 2, 3, 4, 6, 5):
                load(b + 1, i).start()

        def collect(c):
            start, width, _ = chunks[c]
            for o in range(1, n_dp):
                remote(
                    send_b.at[b, dp, :, pl.ds(start, width)],
                    recv_b.at[b, o - 1, :, pl.ds(start, width)],
                    b_send.at[b, c, o], b_recv.at[b, c, o], "dp", peer_dp(o),
                ).wait_recv()
            total = send_b[b, dp, :, start:start + width].astype(F32)
            for o in range(1, n_dp):
                total = total + recv_b[b, o - 1, :, start:start + width].astype(F32)
            return total

        got = collect(0)
        sq = got[:, 3 * kc:3 * kc + 1] + got[:, 3 * kc + LANES:3 * kc + LANES + 1]
        inv = lax.rsqrt(sq / model + 1e-06)
        pre = got[:, :kc] * inv + shift[b:b + 1, :]
        log_sig = jnp.minimum(pre, 0.0) - jnp.log(1.0 + jnp.exp(-jnp.abs(pre)))
        cols[0:pad, :] = jnp.zeros((pad, kc), F32)
        cols[0:seqs, :] = jnp.exp(log_sig[:seqs] / 16.0 + fade[b])
        cols[pad:2 * pad, :] = got[:, kc:2 * kc] * inv
        cols[2 * pad:3 * pad, :] = got[:, 2 * kc:3 * kc] * inv * DK ** (-0.5)
        load(b, 6).wait()
        vals[...] = collect(1) * inv

        for h in range(heads):
            turned = jnp.transpose(cols[:, h * DK:(h + 1) * DK])
            for s in range(seqs):
                dc = turned[:, s:s + 1]
                kcol = turned[:, pad + s:pad + s + 1]
                qc = turned[:, 2 * pad + s:2 * pad + s + 1]
                sl = slice(h * dv, (h + 1) * dv)
                fresh = state[b, s, :, sl] * dc + kcol * vals[s:s + 1, sl]
                state[b, s, :, sl] = fresh
                readout[s:s + 1, sl] = jnp.sum(fresh * qc, axis=0, keepdims=True)
            done = pltpu.make_async_copy(
                state.at[b, :, :, pl.ds(h * dv, dv)], out_hbm.at[b, :, :, pl.ds(h * dv, dv)], out_sem.at[b, h]
            )
            done.start()
            stored.append(done)

        gate = collect(2) * inv
        gated_all[b, dp] = (readout[...] * (gate / (1.0 + jnp.exp(-gate)))).astype(LINK)

        for o in range(1, n_dp):
            copy = remote(gated_all.at[b, dp], gated_all.at[b, dp], d_send.at[b, o], d_recv.at[b, o], "dp", peer_dp(o))
            copy.start()
            sent.append(copy)
        load(b, 5).wait()
        for o in range(1, n_dp):
            src = lax.rem(dp + n_dp - o, n_dp)
            remote(gated_all.at[b, src], gated_all.at[b, src], d_send.at[b, o], d_recv.at[b, o], "dp", src).wait_recv()
        gathered = gated_all[b].astype(F32).reshape(n_dp * pad, vc).astype(jnp.bfloat16)
        part[...] = jnp.dot(gathered, wo[b], preferred_element_type=F32)

        for i in range(n_tp):
            at = pad * (i // per) + rows_tp * (i % per)
            send_e[b, i] = part[at:at + rows_tp, :].astype(LINK)
        for o in range(1, n_tp):
            copy = remote(send_e.at[b, peer_tp(o)], recv_e.at[b, o - 1], e_send.at[b, o], e_recv.at[b, o], "tp", peer_tp(o))
            copy.start()
            sent.append(copy)
        total = send_e[b, tp].astype(F32)
        for o in range(1, n_tp):
            remote(send_e.at[b, tp], recv_e.at[b, o - 1], e_send.at[b, o], e_recv.at[b, o], "tp", peer_tp(o)).wait_recv()
            total = total + recv_e[b, o - 1].astype(F32)
        stream = (resid + total).astype(jnp.bfloat16)
        resid = stream.astype(F32)
        if b + 1 < BLOCKS:
            xg[b + 1, tp] = stream
        else:
            mixed_ref[...] = stream

    for c in sent:
        c.wait_send()
    for c in stored:
        c.wait()


def shards(n_tp, n_dp, x, gain, wq, wk, wf, shift, fade, wv, wg, wo, state):
    rows_tp, depth = x.shape
    kc = wq.shape[2]
    vc = wv.shape[2]
    seqs = state.shape[1]
    heads = kc // DK
    pad = -(-seqs // SUB) * SUB
    width = 3 * kc + 2 * LANES + 2 * vc
    vm = pltpu.VMEM
    dma = pltpu.SemaphoreType.DMA
    anyspec = pl.BlockSpec(memory_space=pl.ANY)
    return pl.pallas_call(
        functools.partial(kernel, n_tp, n_dp),
        out_shape=(
            jax.ShapeDtypeStruct(x.shape, x.dtype),
            jax.ShapeDtypeStruct(state.shape, state.dtype),
        ),
        in_specs=[anyspec] * 11,
        out_specs=(pl.BlockSpec(memory_space=pltpu.VMEM), anyspec),
        scratch_shapes=[
            vm(gain.shape, gain.dtype),
            vm(shift.shape, shift.dtype),
            vm(fade.shape, fade.dtype),
            vm(wq.shape, wq.dtype),
            vm(wk.shape, wk.dtype),
            vm(wf.shape, wf.dtype),
            vm(wv.shape, wv.dtype),
            vm(wg.shape, wg.dtype),
            vm(wo.shape, wo.dtype),
            vm(state.shape, state.dtype),
            vm((BLOCKS, n_tp, rows_tp, depth), x.dtype),
            vm((n_dp * pad, depth), F32),
            vm((BLOCKS, n_dp, pad, width), LINK),
            vm((BLOCKS, n_dp - 1, pad, width), LINK),
            vm((3 * pad, kc), F32),
            vm((pad, vc), F32),
            vm((pad, vc), F32),
            vm((BLOCKS, n_dp, pad, vc), LINK),
            vm((n_dp * pad, wo.shape[2]), F32),
            vm((BLOCKS, n_tp, rows_tp, depth), LINK),
            vm((BLOCKS, n_tp - 1, rows_tp, depth), LINK),
            dma((4,)),
            dma((BLOCKS, 7)),
            dma((BLOCKS, heads)),
            dma((BLOCKS, n_tp)),
            dma((BLOCKS, n_tp)),
            dma((BLOCKS, 3, n_dp)),
            dma((BLOCKS, 3, n_dp)),
            dma((BLOCKS, n_dp)),
            dma((BLOCKS, n_dp)),
            dma((BLOCKS, n_tp)),
            dma((BLOCKS, n_tp)),
        ],
        compiler_params=pltpu.CompilerParams(
            collective_id=0, has_side_effects=True, vmem_limit_bytes=60 * 1024 * 1024
        ),
        name="decode_step",
    )(x, gain, wq, wk, wf, shift, fade, wv, wg, wo, state)


def solution(mesh):
    in_specs = (
        P("tp", "dp"),
        P(None, "dp"),
        P(None, "dp", "tp"),
        P(None, "dp", "tp"),
        P(None, "dp", "tp"),
        P(None, "tp"),
        P(None, "dp", "tp"),
        P(None, "dp", "tp"),
        P(None, "dp", "tp"),
        P(None, "tp", "dp"),
        P(None, "dp", None, "tp"),
    )
    out_specs = (P("tp", "dp"), P(None, "dp", None, "tp"))
    body = functools.partial(shards, mesh.shape["tp"], mesh.shape["dp"])
    return jax.shard_map(body, mesh=mesh, in_specs=in_specs, out_specs=out_specs, check_vma=False)
```

time: 312 us -> 54.7 us (0.18)
  waiting for transfers between devices: 147 us -> 0 us
  blocking collectives: 67.8 us -> 0 us
  Pallas kernels: 0 us -> 44.5 us
  local copies, waits for them, and re-layouts: 40.3 us -> 9.27 us
  other arithmetic: 21.4 us -> 0 us
  matrix products: 19 us -> 0 us
  between operations: 15.3 us -> 0.64 us
    unnamed x8 -> x0, waiting for transfers between devices: 147 us -> none
    all_gather x4 -> x0, blocking collectives: 47.8 us -> none  [the longest x2 31.3 us: shards(): all_rows = lax.all_gather(stream, 'tp', axis=0, tiled=True)]
    pallas_call x0 -> x1, Pallas kernels: none -> 44.5 us  [shards(): pl.pallas_call(functools.partial(kernel, n_tp, n_dp), out_shape=(jax.Shap...]
    psum x2 -> x0, blocking collectives: 20 us -> none  [shards(): total_squares = lax.psum(row_squares, 'dp')]
    dot_general x6 -> x0, matrix products: 19 us -> none  [the longest x2 9.81 us: shards(): jnp.dot(hidden, matrices, preferred_element_type=jnp.float32)]
    another operation x4 -> x0, local copies, waits for them, and re-layouts: 14.2 us -> none  [the longest x2 8.11 us: shards(): memory_tensor[layer_ordinal].reshape(seq_local, DK, heads_here, head_width)]
    add x2 -> x0, other arithmetic: 7.71 us -> none  [shards(): old_state * decays[..., None]]
    another operation x1 -> x0, other arithmetic: 6.68 us -> none  [shards(): return (stream, jnp.stack(collected))]
  transfers between devices with their start and end apart: 4 -> 0, of which waited for: 4 -> 0; matrix products, arithmetic and copies ran while one was open for 8% -> 0% of each run, Pallas kernels for 0% -> 0%
where the time goes in v1:
time: 54.7 us; the launch traced here: 54.5 us
  Pallas kernels  44.5 us (81%)
  local copies, waits for them, and re-layouts  9.27 us (17%)
  between operations  0.64 us (1%)
    pallas_call x1, Pallas kernels, shards(): pl.pallas_call(functools.partial(kernel, n_tp, n_dp), out_shape=(jax.Shap...  44.5 us
    unnamed x3, local copies, waits for them, and re-layouts  9.27 us

profile of v1, /device:TPU:0, one launch (start us, length us, event | category | flops | bytes accessed | tf_op | source)
XLA Modules:
  0.0 54.5 jit_solution(18394906657527183793)
XLA Ops:
  0.6 1.4 %copy.13.fade_hbm = f32[2,6,512]{2,1,0:T(8,128)} copy(f32[2,6,512]{2,0,1:T(2,128)} %param.17) | data formatting | bytes 49152 | tf_op args[6]
  2.0 44.5 %decode_step.1 = (bf16[3,1024]{1,0:T(4,128)(2,1)}, f32[2,6,128,1024]{3,2,1,0:T(8,128)}) custom-call(bf16[3,1024]{1,0:T(4,128)(2,1)} %x_hbm.1, bf16[2,1024]{1,0:T(2,128)(2,1)} %gain_hbm.1, bf16[2,1024,512]{2,1,0:T(8,128)(2,1)} %q_hbm.1, bf16[2,1024,512]{2,1,0:T(8,128)(2,1)} %k_hbm.1, bf16[2,1024,512]{2,1,0:T(8,128)(2,1)} %f_hbm.1, f32[2,512]{1,0:T(2,128)} %shift_hbm.1, ...), custom_call_target="tpu_custom_call" | custom-call | tf_op jit(solution)/shard_map/decode_step/pallas_call | solution.py:226
  46.5 1.3 %copy.16 = bf16[3,1024]{1,0:T(4,128)(2,1)} copy(bf16[3,1024]{1,0:T(4,128)(2,1)} %get-tuple-element.4) | data formatting | bytes 12288
  47.8 6.6 %copy.17 = f32[2,6,128,1024]{3,2,1,0:T(8,128)} copy(f32[2,6,128,1024]{3,2,1,0:T(8,128)} %get-tuple-element.5) | data formatting | bytes 12582912

commit v2 on v1

--- a/solution.py
+++ b/solution.py
@@ -9,6 +9,7 @@
 
 DK = 128
 BLOCKS = 2
+VMEM_BYTES = 67043328
 SUB = 8
 LANES = 128
 LINK = jnp.bfloat16
@@ -17,10 +18,10 @@
 
 def kernel(
     n_tp, n_dp, x_hbm, gain_hbm, q_hbm, k_hbm, f_hbm, shift_hbm, fade_hbm, v_hbm, g_hbm, o_hbm, state_hbm,
-    mixed_ref, out_hbm,
-    gain, shift, fade, wq, wk, wf, wv, wg, wo, state,
+    mixed_ref, state,
+    gain, shift, fade, wq, wk, wf, wv, wg, wo,
     xg, hid, send_b, recv_b, cols, vals, readout, gated_all, part, send_e, recv_e,
-    misc_sem, w_sem, out_sem, a_send, a_recv, b_send, b_recv, d_send, d_recv, e_send, e_recv,
+    misc_sem, w_sem, a_send, a_recv, b_send, b_recv, d_send, d_recv, e_send, e_recv,
 ):
     tp = lax.axis_index("tp")
     dp = lax.axis_index("dp")
@@ -31,6 +32,7 @@
     seqs = state_hbm.shape[1]
     heads = kc // DK
     dv = vc // heads
+    groups = 2 if heads % 2 == 0 else 1
     per = seqs // rows_tp
     pad = hid.shape[0] // n_dp
     model = depth * n_dp
@@ -67,6 +69,7 @@
         pl.semaphore_signal(barrier, inc=1, device_id={"dp": peer_dp(o)}, device_id_type=pl.DeviceIdType.MESH)
     hid[...] = jnp.zeros_like(hid)
     readout[...] = jnp.zeros_like(readout)
+    cols[...] = jnp.zeros_like(cols)
     misc[0].wait()
     misc[1].wait()
     pl.semaphore_wait(barrier, n_tp + n_dp - 2)
@@ -78,7 +81,6 @@
         )
 
     sent = []
-    stored = []
     resid = None
     for b in range(BLOCKS):
         for o in range(1, n_tp):
@@ -104,17 +106,28 @@
             for d in range(n_dp):
                 send_b[b, d, :, at:at + value.shape[1]] = value[pad * d:pad * (d + 1)].astype(LINK)
 
-        put(jnp.broadcast_to(sq_hi, (pad * n_dp, LANES)), 3 * kc)
-        put(jnp.broadcast_to(sq_lo, (pad * n_dp, LANES)), 3 * kc + LANES)
-        first = 3 * kc + 2 * LANES
-        chunks = [(0, first, (0, 1, 2)), (first, vc, (3,)), (first + vc, vc, (4,))]
-        for c, (start, width, members) in enumerate(chunks):
-            at = start
-            for m in members:
-                load(b, m).wait()
-                w = weights[m][1]
-                put(jnp.dot(hidden, w[b], preferred_element_type=F32), at)
-                at += w.shape[2]
+        chunks = []
+        at = 0
+        for g in range(groups + 1):
+            start = at
+            if g < groups:
+                ks = slice(g * kc // groups, (g + 1) * kc // groups)
+                vs = slice(g * vc // groups, (g + 1) * vc // groups)
+                plan = [(0, ks), (1, ks), (2, ks), (3, vs)]
+            else:
+                plan = [(4, slice(0, vc))]
+            for m, sl in plan:
+                if g != 1 or groups == 1:
+                    load(b, m).wait()
+                put(jnp.dot(hidden, weights[m][1][b, :, sl], preferred_element_type=F32), at)
+                at += sl.stop - sl.start
+            if g == 0:
+                put(jnp.broadcast_to(sq_hi, (pad * n_dp, LANES)), at)
+                put(jnp.broadcast_to(sq_lo, (pad * n_dp, LANES)), at + LANES)
+                at += 2 * LANES
+            width = at - start
+            c = g
+            chunks.append((start, width))
             for o in range(1, n_dp):
                 copy = remote(
                     send_b.at[b, peer_dp(o), :, pl.ds(start, width)],
@@ -134,7 +147,7 @@
                 load(b + 1, i).start()
 
         def collect(c):
-            start, width, _ = chunks[c]
+            start, width = chunks[c]
             for o in range(1, n_dp):
                 remote(
                     send_b.at[b, dp, :, pl.ds(start, width)],
@@ -146,35 +159,33 @@
                 total = total + recv_b[b, o - 1, :, start:start + width].astype(F32)
             return total
 
-        got = collect(0)
-        sq = got[:, 3 * kc:3 * kc + 1] + got[:, 3 * kc + LANES:3 * kc + LANES + 1]
-        inv = lax.rsqrt(sq / model + 1e-06)
-        pre = got[:, :kc] * inv + shift[b:b + 1, :]
-        log_sig = jnp.minimum(pre, 0.0) - jnp.log(1.0 + jnp.exp(-jnp.abs(pre)))
-        cols[0:pad, :] = jnp.zeros((pad, kc), F32)
-        cols[0:seqs, :] = jnp.exp(log_sig[:seqs] / 16.0 + fade[b])
-        cols[pad:2 * pad, :] = got[:, kc:2 * kc] * inv
-        cols[2 * pad:3 * pad, :] = got[:, 2 * kc:3 * kc] * inv * DK ** (-0.5)
-        load(b, 6).wait()
-        vals[...] = collect(1) * inv
-
-        for h in range(heads):
-            turned = jnp.transpose(cols[:, h * DK:(h + 1) * DK])
-            for s in range(seqs):
-                dc = turned[:, s:s + 1]
-                kcol = turned[:, pad + s:pad + s + 1]
-                qc = turned[:, 2 * pad + s:2 * pad + s + 1]
-                sl = slice(h * dv, (h + 1) * dv)
-                fresh = state[b, s, :, sl] * dc + kcol * vals[s:s + 1, sl]
-                state[b, s, :, sl] = fresh
-                readout[s:s + 1, sl] = jnp.sum(fresh * qc, axis=0, keepdims=True)
-            done = pltpu.make_async_copy(
-                state.at[b, :, :, pl.ds(h * dv, dv)], out_hbm.at[b, :, :, pl.ds(h * dv, dv)], out_sem.at[b, h]
-            )
-            done.start()
-            stored.append(done)
-
-        gate = collect(2) * inv
+        kw, vw = kc // groups, vc // groups
+        for g in range(groups):
+            got = collect(g)
+            if g == 0:
+                sq = got[:, 3 * kw + vw:3 * kw + vw + 1] + got[:, 3 * kw + vw + LANES:3 * kw + vw + LANES + 1]
+                inv = lax.rsqrt(sq / model + 1e-06)
+            k0, v0 = g * kw, g * vw
+            pre = got[:, :kw] * inv + shift[b:b + 1, k0:k0 + kw]
+            log_sig = jnp.minimum(pre, 0.0) - jnp.log(1.0 + jnp.exp(-jnp.abs(pre)))
+            cols[0:seqs, k0:k0 + kw] = jnp.exp(log_sig[:seqs] / 16.0 + fade[:, b, k0:k0 + kw])
+            cols[pad:2 * pad, k0:k0 + kw] = got[:, kw:2 * kw] * inv
+            cols[2 * pad:3 * pad, k0:k0 + kw] = got[:, 2 * kw:3 * kw] * inv * DK ** (-0.5)
+            vals[:, v0:v0 + vw] = got[:, 3 * kw:3 * kw + vw] * inv
+            if g == 0:
+                load(b, 6).wait()
+            for h in range(g * heads // groups, (g + 1) * heads // groups):
+                turned = jnp.transpose(cols[:, h * DK:(h + 1) * DK])
+                for s in range(seqs):
+                    dc = turned[:, s:s + 1]
+                    kcol = turned[:, pad + s:pad + s + 1]
+                    qc = turned[:, 2 * pad + s:2 * pad + s + 1]
+                    sl = slice(h * dv, (h + 1) * dv)
+                    fresh = state[b, s, :, sl] * dc + kcol * vals[s:s + 1, sl]
+                    state[b, s, :, sl] = fresh
+                    readout[s:s + 1, sl] = jnp.sum(fresh * qc, axis=0, keepdims=True)
+
+        gate = collect(groups) * inv
         gated_all[b, dp] = (readout[...] * (gate / (1.0 + jnp.exp(-gate)))).astype(LINK)
 
         for o in range(1, n_dp):
@@ -208,29 +219,36 @@
 
     for c in sent:
         c.wait_send()
-    for c in stored:
-        c.wait()
+
+
+def store(mixed_vmem, state_vmem, mixed_hbm, state_hbm, sems):
+    moves = [pltpu.make_async_copy(state_vmem.at[b], state_hbm.at[b], sems.at[b]) for b in range(BLOCKS)]
+    moves.append(pltpu.make_async_copy(mixed_vmem, mixed_hbm, sems.at[BLOCKS]))
+    for move in moves:
+        move.start()
+    for move in moves:
+        move.wait()
 
 
 def shards(n_tp, n_dp, x, gain, wq, wk, wf, shift, fade, wv, wg, wo, state):
+    fade = jnp.swapaxes(fade, 0, 1)
     rows_tp, depth = x.shape
     kc = wq.shape[2]
     vc = wv.shape[2]
     seqs = state.shape[1]
-    heads = kc // DK
     pad = -(-seqs // SUB) * SUB
     width = 3 * kc + 2 * LANES + 2 * vc
     vm = pltpu.VMEM
     dma = pltpu.SemaphoreType.DMA
     anyspec = pl.BlockSpec(memory_space=pl.ANY)
-    return pl.pallas_call(
+    mixed, fresh = pl.pallas_call(
         functools.partial(kernel, n_tp, n_dp),
         out_shape=(
-            jax.ShapeDtypeStruct(x.shape, x.dtype),
-            jax.ShapeDtypeStruct(state.shape, state.dtype),
+            pltpu.VMEM(x.shape, x.dtype),
+            pltpu.VMEM(state.shape, state.dtype),
         ),
         in_specs=[anyspec] * 11,
-        out_specs=(pl.BlockSpec(memory_space=pltpu.VMEM), anyspec),
+        out_specs=(pl.BlockSpec(memory_space=pltpu.VMEM), pl.BlockSpec(memory_space=pltpu.VMEM)),
         scratch_shapes=[
             vm(gain.shape, gain.dtype),
             vm(shift.shape, shift.dtype),
@@ -241,7 +259,6 @@
             vm(wv.shape, wv.dtype),
             vm(wg.shape, wg.dtype),
             vm(wo.shape, wo.dtype),
-            vm(state.shape, state.dtype),
             vm((BLOCKS, n_tp, rows_tp, depth), x.dtype),
             vm((n_dp * pad, depth), F32),
             vm((BLOCKS, n_dp, pad, width), LINK),
@@ -255,7 +272,6 @@
             vm((BLOCKS, n_tp - 1, rows_tp, depth), LINK),
             dma((4,)),
             dma((BLOCKS, 7)),
-            dma((BLOCKS, heads)),
             dma((BLOCKS, n_tp)),
             dma((BLOCKS, n_tp)),
             dma((BLOCKS, 3, n_dp)),
@@ -266,10 +282,25 @@
             dma((BLOCKS, n_tp)),
         ],
         compiler_params=pltpu.CompilerParams(
-            collective_id=0, has_side_effects=True, vmem_limit_bytes=60 * 1024 * 1024
+            collective_id=0, has_side_effects=True, vmem_limit_bytes=VMEM_BYTES - state.size * 4 - (1 << 20)
         ),
         name="decode_step",
     )(x, gain, wq, wk, wf, shift, fade, wv, wg, wo, state)
+    return pl.pallas_call(
+        store,
+        out_shape=(
+            jax.ShapeDtypeStruct(x.shape, x.dtype),
+            jax.ShapeDtypeStruct(state.shape, state.dtype),
+        ),
+        in_specs=[pl.BlockSpec(memory_space=pltpu.VMEM)] * 2,
+        out_specs=(anyspec, anyspec),
+        scratch_shapes=[dma((BLOCKS + 1,))],
+        compiler_params=pltpu.CompilerParams(vmem_limit_bytes=1 << 20),
+        name="store_results",
+    )(
+        pltpu.with_memory_space_constraint(mixed, pltpu.VMEM),
+        pltpu.with_memory_space_constraint(fresh, pltpu.VMEM),
+    )
 
 
 def solution(mesh):

time: 54.7 us -> 46.8 us (0.86)
  local copies, waits for them, and re-layouts: 9.27 us -> 0 us
  Pallas kernels: 44.5 us -> 46 us
    unnamed x3 -> x0, local copies, waits for them, and re-layouts: 9.27 us -> none
    pallas_call x1 -> x2, Pallas kernels: 44.5 us -> 46 us  [the longest x1 43.3 us: shards(): pl.pallas_call(functools.partial(kernel, n_tp, n_dp), out_shape=(pltpu.VM...]
where the time goes in v2:
time: 46.8 us; the launch traced here: 46.6 us
  Pallas kernels  46 us (98%)
  between operations  0.64 us (1%)
    pallas_call x1, Pallas kernels, shards(): pl.pallas_call(functools.partial(kernel, n_tp, n_dp), out_shape=(pltpu.VM...  43.3 us
    pallas_call x1, Pallas kernels, shards(): pl.pallas_call(store, out_shape=(jax.ShapeDtypeStruct(x.shape, x.dtype),...  2.73 us

profile of v2, /device:TPU:0, one launch (start us, length us, event | category | flops | bytes accessed | tf_op | source)
XLA Modules:
  0.0 46.6 jit_solution(16197916181936107449)
XLA Ops:
  0.6 43.3 %decode_step.1 = (bf16[3,1024]{1,0:T(4,128)(2,1)S(1)}, f32[2,6,128,1024]{3,2,1,0:T(8,128)S(1)}) custom-call(bf16[3,1024]{1,0:T(4,128)(2,1)} %x_hbm.1, bf16[2,1024]{1,0:T(2,128)(2,1)} %gain_hbm.1, bf16[2,1024,512]{2,1,0:T(8,128)(2,1)} %q_hbm.1, bf16[2,1024,512]{2,1,0:T(8,128)(2,1)} %k_hbm.1, bf16[2,1024,512]{2,1,0:T(8,128)(2,1)} %f_hbm.1, ...), custom_call_target="tpu_custom_call" | custom-call | tf_op jit(solution)/shard_map/decode_step/pallas_call | solution.py:244
  43.9 2.7 %store_results.1 = (bf16[3,1024]{1,0:T(4,128)(2,1)}, f32[2,6,128,1024]{3,2,1,0:T(8,128)}) custom-call(bf16[3,1024]{1,0:T(4,128)(2,1)S(1)} %get-tuple-element.4.mixed_vmem, f32[2,6,128,1024]{3,2,1,0:T(8,128)S(1)} %get-tuple-element.5.state_vmem), custom_call_target="tpu_custom_call" | custom-call | tf_op jit(solution)/shard_map/store_results/pallas_call | solution.py:289
